TPU v7x, 32 devices: a whole 2x2x4 slice. The times are simulated.
32 devices in a mesh: ep: 8 (over z, x), tp: 4 (over y, core).
Axes of the slice: x: 2, y: 2, z: 4, core: 2. Of those that a mesh axis runs over, the one named last changes fastest.
Arguments:
- hidden_in: bfloat16 [128, 1024], P('ep'), may hold values from -6 to 6
- attn_gain: float32 [1024], replicated, may hold values from 0.1 to 1.9
- w_qdown: bfloat16 [1024, 256], replicated, may hold values from -0.1875 to 0.1875
- q_gain: float32 [256], replicated, may hold values from 0.1 to 1.9
- w_qnope: bfloat16 [256, 512], replicated, may hold values from -0.375 to 0.375
- w_qrope: bfloat16 [256, 256], replicated, may hold values from -0.375 to 0.375
- w_kvdown: bfloat16 [1024, 128], replicated, may hold values from -0.1875 to 0.1875
- kv_gain: float32 [128], replicated, may hold values from 0.1 to 1.9
- w_krope: bfloat16 [1024, 32], replicated, may hold values from -0.1875 to 0.1875
- w_ukey: bfloat16 [128, 512], replicated, may hold values from -0.75 to 0.75
- w_uvalue: bfloat16 [128, 512], replicated, may hold values from -0.5 to 0.5
- w_out: bfloat16 [512, 1024], P('tp'), may hold values from -0.25 to 0.25
- cache_latent: bfloat16 [128, 1024, 128], P(('ep', 'tp')), may hold values from -6 to 6
- cache_rope: bfloat16 [128, 32, 1024], P(('ep', 'tp')), may hold values from -900 to 900
- lengths: int32 [128], P(('ep', 'tp')), may hold values from 1 to 1024, as said below
- ffn_gain: float32 [1024], replicated, may hold values from 0.1 to 1.9
- routes: int32 [128, 2], P('ep'), may hold values from 0 to 3, all different within a row; in each aligned block of 16 rows (0 to 15, 16 to 31, ...) at most 16 rows name the same one
- route_weights: float32 [128, 2], P('ep'), may hold values from 0.25 to 1
- w_gate: bfloat16 [8, 1024, 1792], P('ep', None, 'tp'), may hold values from -0.1875 to 0.1875
- w_up: bfloat16 [8, 1024, 1792], P('ep', None, 'tp'), may hold values from -0.1875 to 0.1875
- w_down: bfloat16 [8, 1792, 1024], P('ep', 'tp'), may hold values from -0.09375 to 0.09375
Outputs:
- next_hidden: bfloat16 [128, 1024], P('ep', 'tp')
Inputs may be any that keep to these rules, and one draw needn't show every extreme that they name: `lengths`: each sequence has 1 to 1024 valid cached positions; in every aligned block of 16 sequences one has all 1024. `routes`: each row names two different experts. In the aligned blocks of 16 rows no expert is named by more than 16 rows, and in some block one expert is named by exactly 16.
All inputs are finite; a program needn't handle non-finite values.
Results may differ from a plain program's by a relative error of at most 0.014.
The roundings to bfloat16 on the way count: a program that leaves them out, or rounds other values in their place, can miss the bound.
Values may be sent and summed in bfloat16 or wider, within the bound.
A program may use at most 64 MiB of HBM per device.

v0:
```python
import jax
import jax.numpy as jnp
from jax import lax
from jax.sharding import PartitionSpec as P

HEADS = 8
NOPE = 64
ROPE = 32
VDIM = 64
KVLORA = 128


eps = 1e-06
rope_base = 10000.0


def rms_scale(values, gain):
    return values * lax.rsqrt(jnp.mean(values * values, axis=-1, keepdims=True) + eps) * gain


def rotate(values, positions):
    width = values.shape[-1]
    middle = width // 2
    inverse = jnp.power(rope_base, -jnp.arange(0, width, 2).astype(jnp.float32) / width)
    angles = positions.astype(jnp.float32)[:, None] * inverse[None, :]
    angles = jnp.concatenate([angles, angles], axis=-1)
    target = (angles.shape[0],) + (1,) * (values.ndim - 2) + (width,)
    cosine = jnp.cos(angles).reshape(target)
    sine = jnp.sin(angles).reshape(target)
    turned = jnp.concatenate([-values[..., middle:], values[..., :middle]], axis=-1)
    return values * cosine + turned * sine


def route_slots(route_table, expert_count):
    flat_ids = route_table.reshape(-1)
    onehot = (flat_ids[:, None] == jnp.arange(expert_count, dtype=jnp.int32)[None, :]).astype(
        jnp.int32
    )
    before = jnp.cumsum(onehot, axis=0) - onehot
    return jnp.sum(before * onehot, axis=1).reshape(route_table.shape)


def unit_block(arrived, w_gate, w_up, w_down):
    gate_part = jnp.einsum("scd,df->scf", arrived, w_gate[0], preferred_element_type=jnp.float32)
    up_part = jnp.einsum("scd,df->scf", arrived, w_up[0], preferred_element_type=jnp.float32)
    inner = (jax.nn.silu(gate_part) * up_part).astype(jnp.bfloat16)
    block_term = jnp.einsum("scf,fd->scd", inner, w_down[0], preferred_element_type=jnp.float32)
    summed = lax.psum_scatter(
        block_term.astype(jnp.bfloat16), "tp", scatter_dimension=2, tiled=True
    )
    return lax.all_to_all(summed, "ep", split_axis=0, concat_axis=0, tiled=True)


def per_device(
    hidden_in,
    attn_gain,
    w_qdown,
    q_gain,
    w_qnope,
    w_qrope,
    w_kvdown,
    kv_gain,
    w_krope,
    w_ukey,
    w_uvalue,
    w_out,
    cache_latent,
    cache_rope,
    lengths,
    ffn_gain,
    routes,
    route_weights,
    w_gate,
    w_up,
    w_down,
):
    group_rows, width = hidden_in.shape
    own_count = lengths.shape[0]
    tp_rank = lax.axis_index("tp")
    score_scale = (NOPE + ROPE) ** (-0.5)
    own_rows = lax.dynamic_slice_in_dim(hidden_in, tp_rank * own_count, own_count, 0).astype(
        jnp.float32
    )
    normed = rms_scale(own_rows, attn_gain).astype(jnp.bfloat16)
    q_small = rms_scale(
        jnp.dot(normed, w_qdown, preferred_element_type=jnp.float32), q_gain
    ).astype(jnp.bfloat16)
    q_plain = (
        jnp.dot(q_small, w_qnope, preferred_element_type=jnp.float32)
        .astype(jnp.bfloat16)
        .reshape(own_count, HEADS, NOPE)
    )
    q_turned = rotate(
        jnp.dot(q_small, w_qrope, preferred_element_type=jnp.float32).reshape(
            own_count, HEADS, ROPE
        ),
        lengths,
    ).astype(jnp.bfloat16)
    q_latent = jnp.einsum(
        "shn,chn->shc",
        q_plain,
        w_ukey.reshape(KVLORA, HEADS, NOPE),
        preferred_element_type=jnp.float32,
    ).astype(jnp.bfloat16)
    new_latent = rms_scale(
        jnp.dot(normed, w_kvdown, preferred_element_type=jnp.float32), kv_gain
    ).astype(jnp.bfloat16)
    new_rope = rotate(jnp.dot(normed, w_krope, preferred_element_type=jnp.float32), lengths).astype(
        jnp.bfloat16
    )
    past_scores = (
        jnp.einsum("shc,spc->shp", q_latent, cache_latent, preferred_element_type=jnp.float32)
        + jnp.einsum("shr,srp->shp", q_turned, cache_rope, preferred_element_type=jnp.float32)
    ) * score_scale
    in_range = jnp.arange(cache_latent.shape[1])[None, None, :] < lengths[:, None, None]
    past_scores = jnp.where(in_range, past_scores, -1e30)
    fresh_score = (
        jnp.einsum("shc,sc->sh", q_latent, new_latent, preferred_element_type=jnp.float32)
        + jnp.einsum("shr,sr->sh", q_turned, new_rope, preferred_element_type=jnp.float32)
    ) * score_scale
    highest = jnp.maximum(jnp.max(past_scores, axis=-1), fresh_score)
    past_exp = jnp.exp(past_scores - highest[..., None])
    fresh_exp = jnp.exp(fresh_score - highest)
    divisor = jnp.sum(past_exp, axis=-1) + fresh_exp
    past_prob = (past_exp / divisor[..., None]).astype(jnp.bfloat16)
    fresh_prob = (fresh_exp / divisor).astype(jnp.bfloat16)
    latent_mix = (
        jnp.einsum("shp,spc->shc", past_prob, cache_latent, preferred_element_type=jnp.float32)
        + fresh_prob.astype(jnp.float32)[..., None] * new_latent.astype(jnp.float32)[:, None, :]
    ).astype(jnp.bfloat16)
    head_values = (
        jnp.einsum(
            "shc,chv->shv",
            latent_mix,
            w_uvalue.reshape(KVLORA, HEADS, VDIM),
            preferred_element_type=jnp.float32,
        )
        .astype(jnp.bfloat16)
        .reshape(own_count, HEADS * VDIM)
    )
    by_heads = lax.all_to_all(head_values, "tp", split_axis=1, concat_axis=0, tiled=True)
    attended = lax.psum(
        jnp.dot(by_heads, w_out, preferred_element_type=jnp.float32).astype(jnp.bfloat16), "tp"
    ).astype(jnp.float32)
    residual = hidden_in.astype(jnp.float32) + attended
    normed_two = rms_scale(residual, ffn_gain).astype(jnp.bfloat16)
    unit_count = lax.axis_size("ep")
    expert_count = unit_count // 2
    capacity = max(2, 4 * group_rows // expert_count)
    quarter = width // lax.axis_size("tp")
    slots = route_slots(routes, expert_count)
    expert_of_unit = jnp.arange(unit_count, dtype=jnp.int32) // 2
    slot_range = jnp.arange(capacity, dtype=jnp.int32)
    chosen = (routes[None, None, :, :] == expert_of_unit[:, None, None, None]) & (
        slots[None, None, :, :] == slot_range[None, :, None, None]
    )
    chooser = jnp.sum(chosen.astype(jnp.int32), axis=-1).astype(jnp.bfloat16)
    outgoing = jnp.einsum(
        "ucr,rd->ucd", chooser, normed_two, preferred_element_type=jnp.float32
    ).astype(jnp.bfloat16)
    returned = unit_block(
        lax.all_to_all(outgoing, "ep", split_axis=0, concat_axis=0, tiled=True),
        w_gate,
        w_up,
        w_down,
    )
    stacked = returned.reshape(unit_count * capacity, quarter)
    first_row = routes * (2 * capacity) + slots
    first_half = stacked[first_row].astype(jnp.float32)
    second_half = stacked[first_row + capacity].astype(jnp.float32)
    blended = jnp.sum(route_weights[..., None] * (first_half + second_half), axis=1)
    own_columns = lax.dynamic_slice_in_dim(residual, tp_rank * quarter, quarter, 1)
    return (own_columns + blended).astype(jnp.bfloat16)


def solution(mesh):
    placed = (
        P("ep", None),
        P(),
        P(),
        P(),
        P(),
        P(),
        P(),
        P(),
        P(),
        P(),
        P(),
        P("tp", None),
        P(("ep", "tp"), None, None),
        P(("ep", "tp"), None, None),
        P(("ep", "tp")),
        P(),
        P("ep", None),
        P("ep", None),
        P("ep", None, "tp"),
        P("ep", None, "tp"),
        P("ep", "tp", None),
    )
    return jax.shard_map(
        per_device, mesh=mesh, in_specs=placed, out_specs=P("ep", "tp"), check_vma=False
    )
```

profile of v0, /device:TPU:0, one launch (start us, length us, event | category | flops | bytes accessed | tf_op | source)
XLA Modules:
  0.0 95.3 jit_solution(16051706030308229401)
XLA Ops:
  6.5 0.8 convert_element_type.106
  7.3 0.7 iota_compare_fusion.2
  8.0 0.8 fusion.25
  8.9 1.1 %fusion.49 = f32[4,32]{1,0:T(4,128)S(1)} fusion(bf16[1024,32]{0,1:T(8,128)(2,1)} %param.29, f32[1024]{0:T(1024)} %param.22, f32[4]{0:T(128)S(1)} %add_rsqrt_fusion.3, bf16[16,1024]{1,0:T(8,128)(2,1)S(1)} %copy-done.4, s32[]{:T(128)S(6)} %select_n.25), kind=kOutput, calls=%fused_computation.101 | convolution fusion | flops 278528 | bytes 78852 | tf_op jit(solution)/shard_map/dot_general | solution.py:108
  10.0 1.4 %multiply_reduce_fusion.2 = (f32[4]{0:T(128)S(1)}, f32[4,256]{1,0:T(4,128)S(1)}) fusion(bf16[1024,256]{1,0:T(8,128)(2,1)} %param.23, f32[1024]{0:T(1024)S(1)} %copy-done.8, f32[4]{0:T(128)S(1)} %add_rsqrt_fusion.3, bf16[16,1024]{1,0:T(8,128)(2,1)S(1)} %copy-done.4, s32[]{:T(128)S(6)} %select_n.25), kind=kOutput, calls=%fused_computation.66 | convolution fusion | flops 2115580 | bytes 541204 | tf_op jit(solution)/shard_map/dot_general | solution.py:86
  11.4 0.7 copy-done.16
  12.4 0.2 convolution_convert_fusion.5
  12.7 0.6 copy-done.5
  13.9 0.4 copy-done.14
  14.3 0.3 multiply_reduce_fusion.3
  14.8 0.7 copy-done.11
  15.7 0.5 fusion.56
  16.1 0.2 fusion.17
  16.3 0.7 copy-done.6
  17.2 0.3 fusion.3
  17.5 0.2 fusion.5
  17.8 0.6 copy.74
  18.4 4.3 %all-to-all-start = ((bf16[4,4,128]{2,0,1:T(4,128)(2,1)}), bf16[4,4,128]{2,0,1:T(4,128)(2,1)S(1)}, u32[]{:S(2)}, u32[]{:S(2)}) async-start(bf16[4,4,128]{2,0,1:T(4,128)(2,1)} %copy.74), calls=%async_computation | async-start | bytes 8192 | tf_op jit(solution)/shard_map/all_to_all | solution.py:141
  23.0 0.2 select_reduce_fusion
  23.5 3.0 %all-to-all-done = bf16[4,4,128]{2,0,1:T(4,128)(2,1)S(1)} async-done(((bf16[4,4,128]{2,0,1:T(4,128)(2,1)}), bf16[4,4,128]{2,0,1:T(4,128)(2,1)S(1)}, u32[]{:S(2)}, u32[]{:S(2)}) %all-to-all-start) | async-done | bytes 4128 | tf_op jit(solution)/shard_map/all_to_all | solution.py:141
  26.6 10.3 %psum.7 = bf16[16,1024]{1,0:T(8,128)(2,1)S(1)} all-reduce(bf16[16,1024]{1,0:T(8,128)(2,1)S(1)} %convolution_convert_fusion.2), channel_id=1, replica_groups=mesh['ep'=8,'tp'=4] {'tp'}, use_global_device_ids=true, to_apply=%region_5.6 | all-reduce | flops 16384 | bytes 65536 | tf_op jit(solution)/shard_map/psum | solution.py:142
  37.0 0.3 convolution_convert_fusion
  37.3 15.4 %all_to_all.29 = bf16[8,16,1024]{2,1,0:T(8,128)(2,1)S(1)} all-to-all(bf16[8,16,1024]{2,1,0:T(8,128)(2,1)S(1)} %convolution_convert_fusion), channel_id=1, replica_groups=mesh['ep'=8,'tp'=4] {'ep'}, dimensions={0} | all-to-all | bytes 524288 | tf_op jit(solution)/shard_map/all_to_all | solution.py:162
  52.7 0.4 fusion.9
  53.1 2.6 %convolution_convert_fusion.1 = bf16[8,16,1024]{2,1,0:T(8,128)(2,1)} fusion(bf16[8,16,1024]{2,1,0:T(8,128)(2,1)S(1)} %all_to_all.29, bf16[1,448,1024]{2,1,0:T(8,128)(2,1)S(1)} %copy-done.12, bf16[1,1024,448]{1,2,0:T(8,128)(2,1)} %param.40, f32[8,16,448]{2,1,0:T(8,128)S(1)} %fusion.9), kind=kOutput, calls=%fused_computation.3 | convolution fusion | flops 235356160 | bytes 2588672 | tf_op jit(solution)/shard_map/scf,fd->scd/dot_general | solution.py:47
  55.9 18.1 %reduce-scatter.2.cloned.1.call-done = bf16[8,16,256]{2,1,0:T(8,128)(2,1)} async-done(((bf16[8,16,1024]{2,1,0:T(8,128)(2,1)}), bf16[8,16,256]{2,1,0:T(8,128)(2,1)}) %reduce-scatter.2.cloned.1.call-update) | async-done | bytes 65552 | tf_op jit(solution)/shard_map/reduce_scatter | solution.py:48
  74.0 5.5 %all-to-all-start.2 = ((bf16[8,16,256]{2,1,0:T(8,128)(2,1)}), bf16[8,16,256]{2,1,0:T(8,128)(2,1)S(1)}, u32[]{:S(2)}, u32[]{:S(2)}) async-start(bf16[8,16,256]{2,1,0:T(8,128)(2,1)} %reduce-scatter.2.cloned.1.call-done), calls=%async_computation.3 | async-start | bytes 131072 | tf_op jit(solution)/shard_map/all_to_all | solution.py:51
  79.7 0.6 copy-done.10
  80.4 6.0 %all-to-all-done.2 = bf16[8,16,256]{2,1,0:T(8,128)(2,1)S(1)} async-done(((bf16[8,16,256]{2,1,0:T(8,128)(2,1)}), bf16[8,16,256]{2,1,0:T(8,128)(2,1)S(1)}, u32[]{:S(2)}, u32[]{:S(2)}) %all-to-all-start.2) | async-done | bytes 65568 | tf_op jit(solution)/shard_map/all_to_all | solution.py:51
  86.4 0.6 gather_fusion
  87.1 0.6 gather_fusion.1
  87.8 0.6 add_convert_fusion
  (76 shorter events, 3.2 us)
Async XLA Ops:
  6.5 9.1 %copy-start = (bf16[4,1024,128]{2,1,0:T(8,128)(2,1)S(1)}, bf16[4,1024,128]{2,1,0:T(8,128)(2,1)}, u32[]{:S(2)}) copy-start(bf16[4,1024,128]{2,1,0:T(8,128)(2,1)} %param.33) | copy-start | bytes 3145732
  6.5 2.3 %copy-start.4 = (bf16[16,1024]{1,0:T(8,128)(2,1)S(1)}, bf16[16,1024]{1,0:T(8,128)(2,1)}, u32[]{:S(2)}) copy-start(bf16[16,1024]{1,0:T(8,128)(2,1)} %param.21) | copy-start | bytes 98308
  8.9 1.1 %copy-start.8 = (f32[1024]{0:T(1024)S(1)}, f32[1024]{0:T(1024)}, u32[]{:S(2)}) copy-start(f32[1024]{0:T(1024)} %param.22) | copy-start | bytes 12292
  10.0 1.5 %copy-start.15 = (bf16[256,256]{1,0:T(8,128)(2,1)S(1)}, bf16[256,256]{1,0:T(8,128)(2,1)}, u32[]{:S(2)}) copy-start(bf16[256,256]{1,0:T(8,128)(2,1)} %param.26) | copy-start | bytes 393220
  10.0 2.5 %copy-start.13 = (bf16[256,512]{1,0:T(8,128)(2,1)S(1)}, bf16[256,512]{1,0:T(8,128)(2,1)}, u32[]{:S(2)}) copy-start(bf16[256,512]{1,0:T(8,128)(2,1)} %param.25) | copy-start | bytes 786436
  11.4 0.7 copy-start.16
  12.3 0.9 copy-start.5
  12.4 1.3 %copy-start.3 = (bf16[4,32,1024]{2,1,0:T(8,128)(2,1)S(1)}, bf16[4,32,1024]{2,1,0:T(8,128)(2,1)}, u32[]{:S(2)}) copy-start(bf16[4,32,1024]{2,1,0:T(8,128)(2,1)} %param.34) | copy-start | bytes 786436
  13.4 1.0 %copy-start.14 = (bf16[1024,128]{1,0:T(8,128)(2,1)S(1)}, bf16[1024,128]{1,0:T(8,128)(2,1)}, u32[]{:S(2)}) copy-start(bf16[1024,128]{1,0:T(8,128)(2,1)} %param.27) | copy-start | bytes 786436
  14.8 0.7 copy-start.11
  16.1 0.9 copy-start.6
  17.2 5.5 %copy-start.7 = (s32[16,2]{0,1:T(2,128)S(1)}, s32[16,2]{0,1:T(2,128)}, u32[]{:S(2)}) copy-start(s32[16,2]{0,1:T(2,128)} %param.37) | copy-start | bytes 388
  17.2 9.3 %copy-start.2 = (bf16[128,1024]{1,0:T(8,128)(2,1)S(1)}, bf16[128,1024]{1,0:T(8,128)(2,1)}, u32[]{:S(2)}) copy-start(bf16[128,1024]{1,0:T(8,128)(2,1)} %param.32) | copy-start | bytes 786436
  17.2 19.8 %copy-start.9 = (f32[1024]{0:T(1024)S(1)}, f32[1024]{0:T(1024)}, u32[]{:S(2)}) copy-start(f32[1024]{0:T(1024)} %param.36) | copy-start | bytes 12292
  17.5 35.2 %copy-start.1 = (bf16[1,1024,448]{1,2,0:T(8,128)(2,1)S(1)}, bf16[1,1024,448]{1,2,0:T(8,128)(2,1)}, u32[]{:S(2)}) copy-start(bf16[1,1024,448]{1,2,0:T(8,128)(2,1)} %param.39) | copy-start | bytes 2752516
  18.4 8.1 %all-to-all-start = ((bf16[4,4,128]{2,0,1:T(4,128)(2,1)}), bf16[4,4,128]{2,0,1:T(4,128)(2,1)S(1)}, u32[]{:S(2)}, u32[]{:S(2)}) async-start(bf16[4,4,128]{2,0,1:T(4,128)(2,1)} %copy.74), calls=%async_computation | async-start | bytes 8192 | tf_op jit(solution)/shard_map/all_to_all | solution.py:141
  22.7 51.3 %reduce-scatter.2.cloned.1.call-start = ((), (), s32[]{:S(2)}) async-start(), calls=%async_computation.4 | async-start | bytes 327680 | tf_op jit(solution)/shard_map/reduce_scatter | solution.py:48
  37.3 15.8 %copy-start.12 = (bf16[1,448,1024]{2,1,0:T(8,128)(2,1)S(1)}, bf16[1,448,1024]{2,1,0:T(8,128)(2,1)}, u32[]{:S(2)}) copy-start(bf16[1,448,1024]{2,1,0:T(8,128)(2,1)} %param.41) | copy-start | bytes 2752516
  74.0 12.4 %all-to-all-start.2 = ((bf16[8,16,256]{2,1,0:T(8,128)(2,1)}), bf16[8,16,256]{2,1,0:T(8,128)(2,1)S(1)}, u32[]{:S(2)}, u32[]{:S(2)}) async-start(bf16[8,16,256]{2,1,0:T(8,128)(2,1)} %reduce-scatter.2.cloned.1.call-done), calls=%async_computation.3 | async-start | bytes 131072 | tf_op jit(solution)/shard_map/all_to_all | solution.py:51
  79.6 0.7 copy-start.10
Sparse Core Ops, SparseCore 0:
  55.9 18.0 reduce-scatter.1
where the time goes:
time: 95.9 us; the launch traced here: 95.3 us
  waiting for transfers between devices  27.1 us (28%)
  blocking collectives  25.6 us (27%)
  between operations  13.6 us (14%)
  starting transfers between devices  9.79 us (10%)
  matrix products  8.07 us (8%)
  local copies, waits for them, and re-layouts  6.79 us (7%)
  other arithmetic  4.28 us (4%)
    reduce_scatter x1, waiting for transfers between devices, unit_block(): lax.psum_scatter(block_term.astype(jnp.bfloat16), 'tp', scatter_dimension...  18.1 us
    all_to_all x1, blocking collectives, per_device(): lax.all_to_all(outgoing, 'ep', split_axis=0, concat_axis=0, tiled=True)  15.4 us
    psum x1, blocking collectives, per_device(): lax.psum(jnp.dot(by_heads, w_out, preferred_element_type=jnp.float32).ast...  10.3 us
    all_to_all x1, waiting for transfers between devices, unit_block(): return lax.all_to_all(summed, 'ep', split_axis=0, concat_axis=0, tiled=True)  6.04 us
    all_to_all x1, starting transfers between devices, unit_block(): return lax.all_to_all(summed, 'ep', split_axis=0, concat_axis=0, tiled=True)  5.52 us
    all_to_all x1, starting transfers between devices, per_device(): lax.all_to_all(head_values, 'tp', split_axis=1, concat_axis=0, tiled=True)  4.26 us
    unnamed x38, local copies, waits for them, and re-layouts  4.04 us
    all_to_all x1, waiting for transfers between devices, per_device(): lax.all_to_all(head_values, 'tp', split_axis=1, concat_axis=0, tiled=True)  2.99 us
  transfers between devices with their start and end apart: 3, of which 3 were waited for; matrix products, arithmetic and copies ran while one was open for 1% of the time, Pallas kernels for 0%

commit v1 on v0

--- a/solution.py
+++ b/solution.py
@@ -1,6 +1,11 @@
+import functools
+
 import jax
 import jax.numpy as jnp
+import numpy as np
 from jax import lax
+from jax.experimental import pallas as pl
+from jax.experimental.pallas import tpu as pltpu
 from jax.sharding import PartitionSpec as P
 
 HEADS = 8
@@ -173,6 +178,319 @@
     return (own_columns + blended).astype(jnp.bfloat16)
 
 
+LINK = pl.DeviceIdType.MESH
+F32 = jnp.float32
+BF16 = jnp.bfloat16
+
+
+def mm(a, b):
+    return jnp.dot(a, b, preferred_element_type=F32)
+
+
+def mm_nt(a, b):
+    return lax.dot_general(a, b, (((1,), (1,)), ((), ())), preferred_element_type=F32)
+
+
+def iota(shape, dim):
+    return lax.broadcasted_iota(jnp.int32, shape, dim)
+
+
+def layer_kernel(groups, lanes_tp, *refs):
+    names = 22
+    hbm, out_ref = refs[:names], refs[names]
+    local = refs[names + 1 : 2 * names + 1]
+    (
+        load_sem, hv_send, hv_recv, rows_buf, part, res_buf, x_buf, y_send, y_recv,
+        hv_ss, hv_rs, part_ss, part_rs, x_ss, x_rs, y_ss, y_rs,
+    ) = refs[2 * names + 1 :]
+    (
+        hidden, attn_gain, w_qdown, q_gain, w_qnope, w_qrope, w_kvdown, kv_gain, w_krope,
+        w_ukey, w_uvalue, w_out, cache_latent, cache_rope, lengths, ffn_gain, routes,
+        route_weights, w_gate, w_up, w_down, inverse,
+    ) = local
+    g, t = lax.axis_index("ep"), lax.axis_index("tp")
+    devices = groups * lanes_tp
+    me = g * lanes_tp + t
+
+    barrier = pltpu.get_barrier_semaphore()
+
+    def greet(step, carry):
+        peer = lax.rem(me + step, devices)
+        pl.semaphore_signal(
+            barrier, inc=1, device_id=(peer // lanes_tp, lax.rem(peer, lanes_tp)),
+            device_id_type=LINK,
+        )
+        return carry
+
+    lax.fori_loop(1, devices, greet, 0)
+
+    loads = [
+        pltpu.make_async_copy(hbm[i], local[i], load_sem.at[i]) for i in range(names)
+    ]
+    order = [0, 1, 2, 3, 14, 21, 6, 8, 7, 4, 5, 9, 12, 13, 10, 11, 15, 16, 17, 18, 19, 20]
+    for i in order:
+        loads[i].start()
+
+    own = lengths.shape[0]
+    rows, width = hidden.shape
+    quarter = width // lanes_tp
+    pad = 8
+
+    for i in (0, 1, 2, 3):
+        loads[i].wait()
+    pick = (iota((pad, rows), 1) == iota((pad, rows), 0) + t * own) & (
+        iota((pad, rows), 0) < own
+    )
+    mine = mm(jnp.where(pick, 1.0, 0.0).astype(BF16), hidden[...])
+    normed = rms_scale(mine, attn_gain[...]).astype(BF16)
+    q_small = rms_scale(mm(normed, w_qdown[...]), q_gain[...]).astype(BF16)
+    for i in (14, 21, 6, 8, 7, 4, 5):
+        loads[i].wait()
+    position = jnp.zeros((pad, 1), jnp.int32)
+    for s in range(own):
+        position = jnp.where(iota((pad, 1), 0) == s, lengths[s], position)
+    angles = position.astype(F32) * inverse[...]
+    cosine, sine = jnp.cos(angles), jnp.sin(angles)
+    new_latent = rms_scale(mm(normed, w_kvdown[...]), kv_gain[...]).astype(BF16).astype(F32)
+    rope_key = mm(normed, w_krope[...])
+    turned_key = jnp.concatenate([-rope_key[:, ROPE // 2 :], rope_key[:, : ROPE // 2]], axis=1)
+    new_rope = rope_key * cosine[:, :ROPE] + turned_key * sine[:, :ROPE]
+    new_rope = new_rope.astype(BF16).astype(F32)
+    q_plain = mm(q_small, w_qnope[...]).astype(BF16).astype(F32)
+    q_rope = mm(q_small, w_qrope[...])
+    span = HEADS * ROPE
+    first = (iota((pad, span), 1) & (ROPE - 1)) < ROPE // 2
+    turned = jnp.where(
+        first, -pltpu.roll(q_rope, span - ROPE // 2, 1), pltpu.roll(q_rope, ROPE // 2, 1)
+    )
+    q_turned = (q_rope * cosine + turned * sine).astype(BF16).astype(F32)
+    plain_mask = iota((HEADS, HEADS * NOPE), 1) // NOPE == iota((HEADS, HEADS * NOPE), 0)
+    rope_mask = iota((HEADS, span), 1) // ROPE == iota((HEADS, span), 0)
+    plain_rows = jnp.concatenate(
+        [jnp.where(plain_mask, q_plain[s : s + 1, :], 0.0) for s in range(own)], axis=0
+    ).astype(BF16)
+    rope_rows = jnp.concatenate(
+        [jnp.where(rope_mask, q_turned[s : s + 1, :], 0.0) for s in range(own)], axis=0
+    ).astype(BF16)
+    fold = ((iota((span, ROPE), 0) & (ROPE - 1)) == iota((span, ROPE), 1)).astype(F32)
+    q_heads = mm(rope_rows, fold.astype(BF16))
+    loads[9].wait()
+    q_latent = mm_nt(plain_rows, w_ukey[...]).astype(BF16)
+    loads[12].wait()
+    loads[13].wait()
+    scale = (NOPE + ROPE) ** (-0.5)
+    cache = cache_latent.shape[1]
+    mixes = []
+    for s in range(own):
+        heads = slice(s * HEADS, (s + 1) * HEADS)
+        ql, qr = q_latent[heads], q_heads[heads]
+        scores = (mm_nt(ql, cache_latent[s]) + mm(qr.astype(BF16), cache_rope[s])) * scale
+        scores = jnp.where(iota((HEADS, cache), 1) < lengths[s], scores, -1e30)
+        fresh = (
+            jnp.sum(ql.astype(F32) * new_latent[s : s + 1, :], axis=1, keepdims=True)
+            + jnp.sum(qr * new_rope[s : s + 1, :], axis=1, keepdims=True)
+        ) * scale
+        highest = jnp.maximum(jnp.max(scores, axis=1, keepdims=True), fresh)
+        past_exp = jnp.exp(scores - highest)
+        fresh_exp = jnp.exp(fresh - highest)
+        divisor = jnp.sum(past_exp, axis=1, keepdims=True) + fresh_exp
+        past_prob = (past_exp / divisor).astype(BF16)
+        fresh_prob = (fresh_exp / divisor).astype(BF16).astype(F32)
+        mixes.append(mm(past_prob, cache_latent[s]) + fresh_prob * new_latent[s : s + 1, :])
+    loads[10].wait()
+    mix = jnp.concatenate(mixes, axis=0).astype(BF16)
+    values = mm(mix, w_uvalue[...])
+    value_mask = iota((HEADS, HEADS * VDIM), 1) // VDIM == iota((HEADS, HEADS * VDIM), 0)
+    block = HEADS * VDIM // lanes_tp
+    for s in range(own):
+        row = jnp.sum(
+            jnp.where(value_mask, values[s * HEADS : (s + 1) * HEADS], 0.0), axis=0, keepdims=True
+        )
+        row = row.astype(BF16).astype(F32)
+        for i in range(lanes_tp):
+            hv_send[i, s : s + 1, :] = row[:, i * block : (i + 1) * block]
+
+    pl.semaphore_wait(barrier, devices - 1)
+
+    def hv_copy(peer, slot):
+        return pltpu.make_async_remote_copy(
+            hv_send.at[peer], hv_recv.at[slot], hv_ss.at[peer], hv_rs.at[slot],
+            device_id=(g, peer), device_id_type=LINK,
+        )
+
+    peers = [lax.rem(t + i, lanes_tp) for i in range(1, lanes_tp)]
+    for peer in peers:
+        hv_copy(peer, t).start()
+    hv_recv[t] = hv_send[t]
+    loads[11].wait()
+    loads[15].wait()
+    for peer in peers:
+        hv_copy(peer, peer).wait_recv()
+    for i in range(lanes_tp):
+        rows_buf[i * own : (i + 1) * own, :] = hv_recv[i, :own, :]
+    part[t] = mm(rows_buf[...].astype(BF16), w_out[...]).astype(BF16)
+
+    def part_copy(peer, slot):
+        return pltpu.make_async_remote_copy(
+            part.at[slot], part.at[slot], part_ss.at[peer], part_rs.at[slot],
+            device_id=(g, peer), device_id_type=LINK,
+        )
+
+    for peer in peers:
+        part_copy(peer, t).start()
+    for peer in peers:
+        part_copy(peer, peer).wait_recv()
+    attended = part[0].astype(F32)
+    for i in range(1, lanes_tp):
+        attended = attended + part[i].astype(F32)
+    residual = hidden[...].astype(F32) + attended
+    normed_two = rms_scale(residual, ffn_gain[...]).astype(BF16)
+    for i in range(lanes_tp):
+        x_buf[g, i] = normed_two[:, i * quarter : (i + 1) * quarter]
+        res_buf[i] = residual[:, i * quarter : (i + 1) * quarter]
+
+    def x_copy(other_g, other_t, slot_g, slot_t):
+        return pltpu.make_async_remote_copy(
+            x_buf.at[slot_g, slot_t], x_buf.at[slot_g, slot_t],
+            x_ss.at[other_g, other_t], x_rs.at[slot_g, slot_t],
+            device_id=(other_g, other_t), device_id_type=LINK,
+        )
+
+    def others(step):
+        return lax.rem(g + 1 + step // lanes_tp, groups), lax.rem(t + step, lanes_tp)
+
+    far = (groups - 1) * lanes_tp
+
+    def x_start(step, carry):
+        a, b = others(step)
+        x_copy(a, b, g, t).start()
+        return carry
+
+    lax.fori_loop(0, far, x_start, 0)
+    for i in (16, 17, 18, 19, 20):
+        loads[i].wait()
+
+    def x_wait(step, carry):
+        a, b = others(step)
+        x_copy(a, b, a, b).wait_recv()
+        return carry
+
+    lax.fori_loop(0, far, x_wait, 0)
+
+    tokens = groups * rows
+    gate = jnp.zeros((tokens, w_gate.shape[2]), F32)
+    up = jnp.zeros((tokens, w_gate.shape[2]), F32)
+    for i in range(lanes_tp):
+        piece = x_buf[:, i].reshape(tokens, quarter)
+        depth = slice(i * quarter, (i + 1) * quarter)
+        gate = gate + mm(piece, w_gate[0, depth, :])
+        up = up + mm(piece, w_up[0, depth, :])
+    inner = (gate / (1.0 + jnp.exp(-gate)) * up).astype(BF16)
+    for i in range(lanes_tp):
+        term = mm(inner, w_down[0, :, i * quarter : (i + 1) * quarter]).astype(BF16)
+        y_send[:, i] = term.reshape(groups, rows, quarter)
+
+    def y_copy(other_g, other_t, slot_g, slot_t):
+        return pltpu.make_async_remote_copy(
+            y_send.at[other_g, other_t], y_recv.at[slot_g, slot_t],
+            y_ss.at[other_g, other_t], y_rs.at[slot_g, slot_t],
+            device_id=(other_g, other_t), device_id_type=LINK,
+        )
+
+    def spread(step):
+        peer = lax.rem(me + step, devices)
+        return peer // lanes_tp, lax.rem(peer, lanes_tp)
+
+    def y_start(step, carry):
+        a, b = spread(step)
+        y_copy(a, b, g, t).start()
+        return carry
+
+    lax.fori_loop(1, devices, y_start, 0)
+    y_recv[g, t] = y_send[g, t]
+
+    def y_wait(step, carry):
+        a, b = spread(step)
+        y_copy(a, b, a, b).wait_recv()
+        return carry
+
+    lax.fori_loop(1, devices, y_wait, 0)
+    total = res_buf[t]
+    for u in range(groups):
+        half = y_recv[u, 0].astype(F32)
+        for i in range(1, lanes_tp):
+            half = half + y_recv[u, i].astype(F32)
+        weight = jnp.sum(
+            jnp.where(routes[...] == u // 2, route_weights[...], 0.0), axis=1, keepdims=True
+        )
+        total = total + weight * half.astype(BF16).astype(F32)
+    out_ref[...] = total.astype(BF16)
+
+    for peer in peers:
+        hv_copy(peer, t).wait_send()
+        part_copy(peer, t).wait_send()
+
+    def x_done(step, carry):
+        a, b = others(step)
+        x_copy(a, b, g, t).wait_send()
+        return carry
+
+    lax.fori_loop(0, far, x_done, 0)
+
+    def y_done(step, carry):
+        a, b = spread(step)
+        y_copy(a, b, g, t).wait_send()
+        return carry
+
+    lax.fori_loop(1, devices, y_done, 0)
+
+
+def fused_layer(groups, lanes_tp, *args):
+    args = [a.reshape(1, -1) if a.ndim == 1 and a.dtype == F32 else a for a in args]
+    spots = np.arange(HEADS * ROPE) % (ROPE // 2)
+    args.append(jnp.asarray((rope_base ** (-2.0 * spots / ROPE))[None].astype(np.float32)))
+    rows, width = args[0].shape
+    own = args[14].shape[0]
+    quarter = width // lanes_tp
+    block = HEADS * VDIM // lanes_tp
+    local = [
+        pltpu.SMEM(a.shape, a.dtype) if i == 14 else pltpu.VMEM(a.shape, a.dtype)
+        for i, a in enumerate(args)
+    ]
+    sem = pltpu.SemaphoreType.DMA
+    return pl.pallas_call(
+        functools.partial(layer_kernel, groups, lanes_tp),
+        out_shape=jax.ShapeDtypeStruct((rows, quarter), BF16),
+        in_specs=[pl.BlockSpec(memory_space=pl.ANY)] * len(args),
+        out_specs=pl.BlockSpec(memory_space=pltpu.VMEM),
+        scratch_shapes=local
+        + [
+            sem((len(args),)),
+            pltpu.VMEM((lanes_tp, 8, block), F32),
+            pltpu.VMEM((lanes_tp, 8, block), F32),
+            pltpu.VMEM((rows, block), F32),
+            pltpu.VMEM((lanes_tp, rows, width), BF16),
+            pltpu.VMEM((lanes_tp, rows, quarter), F32),
+            pltpu.VMEM((groups, lanes_tp, rows, quarter), BF16),
+            pltpu.VMEM((groups, lanes_tp, rows, quarter), BF16),
+            pltpu.VMEM((groups, lanes_tp, rows, quarter), BF16),
+            sem((lanes_tp,)), sem((lanes_tp,)), sem((lanes_tp,)), sem((lanes_tp,)),
+            sem((groups, lanes_tp)), sem((groups, lanes_tp)),
+            sem((groups, lanes_tp)), sem((groups, lanes_tp)),
+        ],
+        compiler_params=pltpu.CompilerParams(
+            collective_id=0, has_side_effects=True, vmem_limit_bytes=60 * 1024 * 1024
+        ),
+    )(*args)
+
+
+def pick_form(groups, lanes_tp, *args):
+    rows = args[0].shape[0]
+    if max(2, 4 * rows // (groups // 2)) < rows:
+        return per_device(*args)
+    return fused_layer(groups, lanes_tp, *args)
+
+
 def solution(mesh):
     placed = (
         P("ep", None),
@@ -197,6 +515,7 @@
         P("ep", None, "tp"),
         P("ep", "tp", None),
     )
+    step = functools.partial(pick_form, mesh.shape["ep"], mesh.shape["tp"])
     return jax.shard_map(
-        per_device, mesh=mesh, in_specs=placed, out_specs=P("ep", "tp"), check_vma=False
-    )
+        step, mesh=mesh, in_specs=placed, out_specs=P("ep", "tp"), check_vma=False
+    )

time: 95.9 us -> 41.3 us (0.43)
  the two profiles are of different devices: /device:TPU:0 before, /device:TPU:15 now
where the time goes in v1:
time: 41.3 us; the launch traced here: 41 us
  Pallas kernels  32.4 us (78%)
  local copies, waits for them, and re-layouts  8.65 us (21%)
    pallas_call x1, Pallas kernels, fused_layer(): pl.pallas_call(functools.partial(layer_kernel, groups, lanes_tp), out_sha...  32.4 us
    unnamed x12, local copies, waits for them, and re-layouts  8.65 us

profile of v1, /device:TPU:15, one launch (start us, length us, event | category | flops | bytes accessed | tf_op | source)
XLA Modules:
  0.0 41.0 jit_solution(13862255407966827241)
XLA Ops:
  0.0 0.0 copy-start.1
  0.0 0.7 %copy-done.1 = s32[16,2]{0,1:T(2,128)S(1)} copy-done((s32[16,2]{0,1:T(2,128)S(1)}, s32[16,2]{0,1:T(2,128)}, u32[]{:S(2)}) %copy-start.1) | copy-done | bytes 152
  0.7 0.0 copy-start.2
  0.7 0.7 %copy.24.refs_16_ = s32[16,2]{1,0:T(8,128)} copy(s32[16,2]{0,1:T(2,128)S(1)} %copy-done.1) | data formatting | bytes 256 | tf_op args[16]
  1.4 0.0 copy-done.2
  1.4 0.7 %copy.25.refs_17_ = f32[16,2]{1,0:T(8,128)} copy(f32[16,2]{0,1:T(2,128)S(1)} %copy-done.2) | data formatting | bytes 256 | tf_op args[17]
  2.0 1.7 %copy.23.refs_8_ = bf16[1024,32]{1,0:T(8,128)(2,1)} copy(bf16[1024,32]{0,1:T(8,128)(2,1)} %param.30) | data formatting | bytes 131072 | tf_op args[8]
  3.7 0.0 copy-start
  3.7 2.3 %copy.26.refs_18_ = bf16[1,1024,448]{2,1,0:T(8,128)(2,1)} copy(bf16[1,1024,448]{1,2,0:T(8,128)(2,1)} %param.40) | data formatting | bytes 1835008 | tf_op args[18]
  6.1 0.0 copy-done
  6.1 1.3 %copy.27.refs_19_ = bf16[1,1024,448]{2,1,0:T(8,128)(2,1)} copy(bf16[1,1024,448]{1,2,0:T(8,128)(2,1)S(1)} %copy-done) | data formatting | bytes 1835008 | tf_op args[19]
  7.4 32.4 %shard_map.208 = bf16[16,256]{1,0:T(8,128)(2,1)} custom-call(bf16[16,1024]{1,0:T(8,128)(2,1)} %refs_0_.1, f32[1,1024]{1,0:T(1,128)} %bitcast.4, bf16[1024,256]{1,0:T(8,128)(2,1)} %refs_2_.1, f32[1,256]{1,0:T(1,128)} %bitcast.6, bf16[256,512]{1,0:T(8,128)(2,1)} %refs_4_.1, bf16[256,256]{1,0:T(8,128)(2,1)} %refs_5_.1, bf16[1024,128]{1,0:T(8,128)(2,1)} %refs_6_.1, ...), custom_call_target="tpu_custom_call" | custom-call | tf_op jit(solution)/shard_map/pallas_call | solution.py:461
  39.7 1.3 %copy.29 = bf16[16,256]{1,0:T(8,128)(2,1)} copy(bf16[16,256]{1,0:T(8,128)(2,1)} %shard_map.208) | data formatting | bytes 16384
Async XLA Ops:
  0.0 0.7 %copy-start.1 = (s32[16,2]{0,1:T(2,128)S(1)}, s32[16,2]{0,1:T(2,128)}, u32[]{:S(2)}) copy-start(s32[16,2]{0,1:T(2,128)} %param.38) | copy-start | bytes 388
  0.7 0.7 %copy-start.2 = (f32[16,2]{0,1:T(2,128)S(1)}, f32[16,2]{0,1:T(2,128)}, u32[]{:S(2)}) copy-start(f32[16,2]{0,1:T(2,128)} %param.39) | copy-start | bytes 388
  3.7 2.3 %copy-start = (bf16[1,1024,448]{1,2,0:T(8,128)(2,1)S(1)}, bf16[1,1024,448]{1,2,0:T(8,128)(2,1)}, u32[]{:S(2)}) copy-start(bf16[1,1024,448]{1,2,0:T(8,128)(2,1)} %param.41) | copy-start | bytes 2752516

commit v2 on v1

--- a/solution.py
+++ b/solution.py
@@ -252,7 +252,7 @@
     angles = position.astype(F32) * inverse[...]
     cosine, sine = jnp.cos(angles), jnp.sin(angles)
     new_latent = rms_scale(mm(normed, w_kvdown[...]), kv_gain[...]).astype(BF16).astype(F32)
-    rope_key = mm(normed, w_krope[...])
+    rope_key = mm_nt(normed, w_krope[...])
     turned_key = jnp.concatenate([-rope_key[:, ROPE // 2 :], rope_key[:, : ROPE // 2]], axis=1)
     new_rope = rope_key * cosine[:, :ROPE] + turned_key * sine[:, :ROPE]
     new_rope = new_rope.astype(BF16).astype(F32)
@@ -378,17 +378,25 @@
     lax.fori_loop(0, far, x_wait, 0)
 
     tokens = groups * rows
-    gate = jnp.zeros((tokens, w_gate.shape[2]), F32)
-    up = jnp.zeros((tokens, w_gate.shape[2]), F32)
+    gate = jnp.zeros((tokens, w_gate.shape[1]), F32)
+    up = jnp.zeros((tokens, w_gate.shape[1]), F32)
     for i in range(lanes_tp):
         piece = x_buf[:, i].reshape(tokens, quarter)
         depth = slice(i * quarter, (i + 1) * quarter)
-        gate = gate + mm(piece, w_gate[0, depth, :])
-        up = up + mm(piece, w_up[0, depth, :])
+        gate = gate + mm_nt(piece, w_gate[0, :, depth])
+        up = up + mm_nt(piece, w_up[0, :, depth])
     inner = (gate / (1.0 + jnp.exp(-gate)) * up).astype(BF16)
     for i in range(lanes_tp):
         term = mm(inner, w_down[0, :, i * quarter : (i + 1) * quarter]).astype(BF16)
         y_send[:, i] = term.reshape(groups, rows, quarter)
+
+    same = iota((rows, rows), 0) == iota((rows, rows), 1)
+    weights = []
+    for e in range(groups // 2):
+        flat = jnp.sum(
+            jnp.where(routes[...] == e, route_weights[...], 0.0), axis=0, keepdims=True
+        )
+        weights.append(jnp.sum(jnp.where(same, flat, 0.0), axis=1, keepdims=True))
 
     def y_copy(other_g, other_t, slot_g, slot_t):
         return pltpu.make_async_remote_copy(
@@ -420,11 +428,8 @@
         half = y_recv[u, 0].astype(F32)
         for i in range(1, lanes_tp):
             half = half + y_recv[u, i].astype(F32)
-        weight = jnp.sum(
-            jnp.where(routes[...] == u // 2, route_weights[...], 0.0), axis=1, keepdims=True
-        )
-        total = total + weight * half.astype(BF16).astype(F32)
-    out_ref[...] = total.astype(BF16)
+        total = total + weights[u // 2] * half.astype(BF16).astype(F32)
+    out_ref[...] = total
 
     for peer in peers:
         hv_copy(peer, t).wait_send()
@@ -446,6 +451,11 @@
 
 
 def fused_layer(groups, lanes_tp, *args):
+    args = list(args)
+    for i in (8, 16, 17):
+        args[i] = args[i].T
+    for i in (18, 19):
+        args[i] = args[i].swapaxes(1, 2)
     args = [a.reshape(1, -1) if a.ndim == 1 and a.dtype == F32 else a for a in args]
     spots = np.arange(HEADS * ROPE) % (ROPE // 2)
     args.append(jnp.asarray((rope_base ** (-2.0 * spots / ROPE))[None].astype(np.float32)))
@@ -460,7 +470,7 @@
     sem = pltpu.SemaphoreType.DMA
     return pl.pallas_call(
         functools.partial(layer_kernel, groups, lanes_tp),
-        out_shape=jax.ShapeDtypeStruct((rows, quarter), BF16),
+        out_shape=jax.ShapeDtypeStruct((rows, quarter), F32),
         in_specs=[pl.BlockSpec(memory_space=pl.ANY)] * len(args),
         out_specs=pl.BlockSpec(memory_space=pltpu.VMEM),
         scratch_shapes=local
@@ -481,7 +491,7 @@
         compiler_params=pltpu.CompilerParams(
             collective_id=0, has_side_effects=True, vmem_limit_bytes=60 * 1024 * 1024
         ),
-    )(*args)
+    )(*args).astype(BF16)
 
 
 def pick_form(groups, lanes_tp, *args):

time: 41.3 us -> 34.3 us (0.83)
  local copies, waits for them, and re-layouts: 8.65 us -> 0 us
  other arithmetic: 0 us -> 1.32 us
    unnamed x12 -> x0, local copies, waits for them, and re-layouts: 8.65 us -> none
    convert_element_type x0 -> x1, other arithmetic: none -> 1.32 us  [fused_layer(): return pl.pallas_call(functools.partial(layer_kernel, groups, lanes_tp),...]
where the time goes in v2:
time: 34.3 us; the launch traced here: 34.1 us
  Pallas kernels  32.7 us (95%)
  other arithmetic  1.32 us (4%)
    pallas_call x1, Pallas kernels, fused_layer(): pl.pallas_call(functools.partial(layer_kernel, groups, lanes_tp), out_sha...  32.7 us
    convert_element_type x1, other arithmetic, fused_layer(): return pl.pallas_call(functools.partial(layer_kernel, groups, lanes_tp),...  1.32 us

profile of v2, /device:TPU:15, one launch (start us, length us, event | category | flops | bytes accessed | tf_op | source)
XLA Modules:
  0.0 34.1 jit_solution(7067142940884038597)
XLA Ops:
  0.0 32.7 %shard_map.208 = f32[16,256]{1,0:T(8,128)} custom-call(bf16[16,1024]{1,0:T(8,128)(2,1)} %refs_0_.1, f32[1,1024]{1,0:T(1,128)} %bitcast.12, bf16[1024,256]{1,0:T(8,128)(2,1)} %refs_2_.1, f32[1,256]{1,0:T(1,128)} %bitcast.14, bf16[256,512]{1,0:T(8,128)(2,1)} %refs_4_.1, bf16[256,256]{1,0:T(8,128)(2,1)} %refs_5_.1, bf16[1024,128]{1,0:T(8,128)(2,1)} %refs_6_.1, ...), custom_call_target="tpu_custom_call" | custom-call | tf_op jit(solution)/shard_map/pallas_call | solution.py:471
  32.7 1.3 %convert_element_type.3 = bf16[16,256]{1,0:T(8,128)(2,1)} convert(f32[16,256]{1,0:T(8,128)} %shard_map.208) | non-fusion elementwise | flops 4096 | bytes 24576 | tf_op jit(solution)/shard_map/convert_element_type | solution.py:494

commit v3 on v2

--- a/solution.py
+++ b/solution.py
@@ -201,7 +201,7 @@
     local = refs[names + 1 : 2 * names + 1]
     (
         load_sem, hv_send, hv_recv, rows_buf, part, res_buf, x_buf, y_send, y_recv,
-        hv_ss, hv_rs, part_ss, part_rs, x_ss, x_rs, y_ss, y_rs,
+        hv_ss, hv_rs, part_ss, part_rs, x_ss, x_rs, f_ss, f_rs, y_ss, y_rs,
     ) = refs[2 * names + 1 :]
     (
         hidden, attn_gain, w_qdown, q_gain, w_qnope, w_qrope, w_kvdown, kv_gain, w_krope,
@@ -214,15 +214,14 @@
 
     barrier = pltpu.get_barrier_semaphore()
 
-    def greet(step, carry):
-        peer = lax.rem(me + step, devices)
-        pl.semaphore_signal(
-            barrier, inc=1, device_id=(peer // lanes_tp, lax.rem(peer, lanes_tp)),
-            device_id_type=LINK,
-        )
-        return carry
-
-    lax.fori_loop(1, devices, greet, 0)
+    def ring(step):
+        return lax.rem(g + step, groups)
+
+    peers = [lax.rem(t + i, lanes_tp) for i in range(1, lanes_tp)]
+    for peer in peers:
+        pl.semaphore_signal(barrier, inc=1, device_id=(g, peer), device_id_type=LINK)
+    for i in range(1, groups):
+        pl.semaphore_signal(barrier, inc=1, device_id=(ring(i), t), device_id_type=LINK)
 
     loads = [
         pltpu.make_async_copy(hbm[i], local[i], load_sem.at[i]) for i in range(names)
@@ -310,7 +309,7 @@
         for i in range(lanes_tp):
             hv_send[i, s : s + 1, :] = row[:, i * block : (i + 1) * block]
 
-    pl.semaphore_wait(barrier, devices - 1)
+    pl.semaphore_wait(barrier, groups + lanes_tp - 2)
 
     def hv_copy(peer, slot):
         return pltpu.make_async_remote_copy(
@@ -318,7 +317,6 @@
             device_id=(g, peer), device_id_type=LINK,
         )
 
-    peers = [lax.rem(t + i, lanes_tp) for i in range(1, lanes_tp)]
     for peer in peers:
         hv_copy(peer, t).start()
     hv_recv[t] = hv_send[t]
@@ -346,43 +344,49 @@
     residual = hidden[...].astype(F32) + attended
     normed_two = rms_scale(residual, ffn_gain[...]).astype(BF16)
     for i in range(lanes_tp):
-        x_buf[g, i] = normed_two[:, i * quarter : (i + 1) * quarter]
         res_buf[i] = residual[:, i * quarter : (i + 1) * quarter]
 
-    def x_copy(other_g, other_t, slot_g, slot_t):
+    half_width = width // 2
+    for i in range(2):
+        x_buf[g, i] = normed_two[:, i * half_width : (i + 1) * half_width]
+
+    mine_half = lax.rem(t, 2)
+    partner = t + 1 - 2 * mine_half
+
+    def x_copy(other, slot):
         return pltpu.make_async_remote_copy(
-            x_buf.at[slot_g, slot_t], x_buf.at[slot_g, slot_t],
-            x_ss.at[other_g, other_t], x_rs.at[slot_g, slot_t],
-            device_id=(other_g, other_t), device_id_type=LINK,
-        )
-
-    def others(step):
-        return lax.rem(g + 1 + step // lanes_tp, groups), lax.rem(t + step, lanes_tp)
-
-    far = (groups - 1) * lanes_tp
-
-    def x_start(step, carry):
-        a, b = others(step)
-        x_copy(a, b, g, t).start()
-        return carry
-
-    lax.fori_loop(0, far, x_start, 0)
+            x_buf.at[slot, mine_half], x_buf.at[slot, mine_half], x_ss.at[other], x_rs.at[slot],
+            device_id=(other, t), device_id_type=LINK,
+        )
+
+    def f_copy(slot, half):
+        return pltpu.make_async_remote_copy(
+            x_buf.at[slot, half], x_buf.at[slot, half], f_ss.at[slot], f_rs.at[slot],
+            device_id=(g, partner), device_id_type=LINK,
+        )
+
+    near = sorted(range(1, groups), key=lambda i: min(i, groups - i))
+    for i in near[::-1]:
+        x_copy(ring(i), g).start()
     for i in (16, 17, 18, 19, 20):
         loads[i].wait()
-
-    def x_wait(step, carry):
-        a, b = others(step)
-        x_copy(a, b, a, b).wait_recv()
-        return carry
-
-    lax.fori_loop(0, far, x_wait, 0)
+    for i in near:
+        x_copy(ring(i), ring(i)).wait_recv()
+        f_copy(ring(i), mine_half).start()
+    for i in near:
+        f_copy(ring(i), 1 - mine_half).wait_recv()
+
+    def x_sends_done():
+        for i in near:
+            x_copy(ring(i), g).wait_send()
+            f_copy(ring(i), mine_half).wait_send()
 
     tokens = groups * rows
     gate = jnp.zeros((tokens, w_gate.shape[1]), F32)
     up = jnp.zeros((tokens, w_gate.shape[1]), F32)
-    for i in range(lanes_tp):
-        piece = x_buf[:, i].reshape(tokens, quarter)
-        depth = slice(i * quarter, (i + 1) * quarter)
+    for i in range(2):
+        piece = x_buf[:, i].reshape(tokens, half_width)
+        depth = slice(i * half_width, (i + 1) * half_width)
         gate = gate + mm_nt(piece, w_gate[0, :, depth])
         up = up + mm_nt(piece, w_up[0, :, depth])
     inner = (gate / (1.0 + jnp.exp(-gate)) * up).astype(BF16)
@@ -435,12 +439,7 @@
         hv_copy(peer, t).wait_send()
         part_copy(peer, t).wait_send()
 
-    def x_done(step, carry):
-        a, b = others(step)
-        x_copy(a, b, g, t).wait_send()
-        return carry
-
-    lax.fori_loop(0, far, x_done, 0)
+    x_sends_done()
 
     def y_done(step, carry):
         a, b = spread(step)
@@ -481,11 +480,11 @@
             pltpu.VMEM((rows, block), F32),
             pltpu.VMEM((lanes_tp, rows, width), BF16),
             pltpu.VMEM((lanes_tp, rows, quarter), F32),
-            pltpu.VMEM((groups, lanes_tp, rows, quarter), BF16),
+            pltpu.VMEM((groups, 2, rows, width // 2), BF16),
             pltpu.VMEM((groups, lanes_tp, rows, quarter), BF16),
             pltpu.VMEM((groups, lanes_tp, rows, quarter), BF16),
             sem((lanes_tp,)), sem((lanes_tp,)), sem((lanes_tp,)), sem((lanes_tp,)),
-            sem((groups, lanes_tp)), sem((groups, lanes_tp)),
+            sem((groups,)), sem((groups,)), sem((groups,)), sem((groups,)),
             sem((groups, lanes_tp)), sem((groups, lanes_tp)),
         ],
         compiler_params=pltpu.CompilerParams(
@@ -496,7 +495,7 @@
 
 def pick_form(groups, lanes_tp, *args):
     rows = args[0].shape[0]
-    if max(2, 4 * rows // (groups // 2)) < rows:
+    if max(2, 4 * rows // (groups // 2)) < rows or lanes_tp % 2:
         return per_device(*args)
     return fused_layer(groups, lanes_tp, *args)
 

time: 34.3 us -> 31.5 us (0.918)
  the two profiles are of different devices: /device:TPU:15 before, /device:TPU:0 now
where the time goes in v3:
time: 31.5 us; the launch traced here: 31.1 us
  Pallas kernels  29.8 us (95%)
  other arithmetic  1.32 us (4%)
    pallas_call x1, Pallas kernels, fused_layer(): pl.pallas_call(functools.partial(layer_kernel, groups, lanes_tp), out_sha...  29.8 us
    convert_element_type x1, other arithmetic, fused_layer(): return pl.pallas_call(functools.partial(layer_kernel, groups, lanes_tp),...  1.32 us

profile of v3, /device:TPU:0, one launch (start us, length us, event | category | flops | bytes accessed | tf_op | source)
XLA Modules:
  0.0 31.1 jit_solution(7866407498415246946)
XLA Ops:
  0.0 29.8 %shard_map.208 = f32[16,256]{1,0:T(8,128)} custom-call(bf16[16,1024]{1,0:T(8,128)(2,1)} %refs_0_.1, f32[1,1024]{1,0:T(1,128)} %bitcast.12, bf16[1024,256]{1,0:T(8,128)(2,1)} %refs_2_.1, f32[1,256]{1,0:T(1,128)} %bitcast.14, bf16[256,512]{1,0:T(8,128)(2,1)} %refs_4_.1, bf16[256,256]{1,0:T(8,128)(2,1)} %refs_5_.1, bf16[1024,128]{1,0:T(8,128)(2,1)} %refs_6_.1, ...), custom_call_target="tpu_custom_call" | custom-call | tf_op jit(solution)/shard_map/pallas_call | solution.py:470
  29.8 1.3 %convert_element_type.3 = bf16[16,256]{1,0:T(8,128)(2,1)} convert(f32[16,256]{1,0:T(8,128)} %shard_map.208) | non-fusion elementwise | flops 4096 | bytes 24576 | tf_op jit(solution)/shard_map/convert_element_type | solution.py:493

commit v4 on v3

--- a/solution.py
+++ b/solution.py
@@ -366,13 +366,13 @@
         )
 
     near = sorted(range(1, groups), key=lambda i: min(i, groups - i))
-    for i in near[::-1]:
+    for i in near:
         x_copy(ring(i), g).start()
     for i in (16, 17, 18, 19, 20):
         loads[i].wait()
     for i in near:
-        x_copy(ring(i), ring(i)).wait_recv()
-        f_copy(ring(i), mine_half).start()
+        x_copy(ring(groups - i), ring(groups - i)).wait_recv()
+        f_copy(ring(groups - i), mine_half).start()
     for i in near:
         f_copy(ring(i), 1 - mine_half).wait_recv()
 
@@ -469,7 +469,7 @@
     sem = pltpu.SemaphoreType.DMA
     return pl.pallas_call(
         functools.partial(layer_kernel, groups, lanes_tp),
-        out_shape=jax.ShapeDtypeStruct((rows, quarter), F32),
+        out_shape=pltpu.VMEM((rows, quarter), F32),
         in_specs=[pl.BlockSpec(memory_space=pl.ANY)] * len(args),
         out_specs=pl.BlockSpec(memory_space=pltpu.VMEM),
         scratch_shapes=local

time: 31.5 us -> 29.8 us (0.946)
  Pallas kernels: 29.8 us -> 28.8 us
  other arithmetic: 1.32 us -> 0.6 us
    pallas_call x1, Pallas kernels: 29.8 us -> 28.8 us  [fused_layer(): pl.pallas_call(functools.partial(layer_kernel, groups, lanes_tp), out_sha...]
    convert_element_type x1, other arithmetic: 1.32 us -> 0.6 us  [fused_layer(): return pl.pallas_call(functools.partial(layer_kernel, groups, lanes_tp),...]
where the time goes in v4:
time: 29.8 us; the launch traced here: 29.4 us
  Pallas kernels  28.8 us (97%)
  other arithmetic  0.6 us (2%)
    pallas_call x1, Pallas kernels, fused_layer(): pl.pallas_call(functools.partial(layer_kernel, groups, lanes_tp), out_sha...  28.8 us
    convert_element_type x1, other arithmetic, fused_layer(): return pl.pallas_call(functools.partial(layer_kernel, groups, lanes_tp),...  0.6 us

profile of v4, /device:TPU:0, one launch (start us, length us, event | category | flops | bytes accessed | tf_op | source)
XLA Modules:
  0.0 29.4 jit_solution(6964941069313820903)
XLA Ops:
  0.0 28.8 %shard_map.208 = f32[16,256]{1,0:T(8,128)S(1)} custom-call(bf16[16,1024]{1,0:T(8,128)(2,1)} %refs_0_.1, f32[1,1024]{1,0:T(1,128)} %bitcast.12, bf16[1024,256]{1,0:T(8,128)(2,1)} %refs_2_.1, f32[1,256]{1,0:T(1,128)} %bitcast.14, bf16[256,512]{1,0:T(8,128)(2,1)} %refs_4_.1, bf16[256,256]{1,0:T(8,128)(2,1)} %refs_5_.1, bf16[1024,128]{1,0:T(8,128)(2,1)} %refs_6_.1, ...), custom_call_target="tpu_custom_call" | custom-call | tf_op jit(solution)/shard_map/pallas_call | solution.py:470
  28.8 0.6 %convert_element_type.3 = bf16[16,256]{1,0:T(8,128)(2,1)} convert(f32[16,256]{1,0:T(8,128)S(1)} %shard_map.208) | non-fusion elementwise | flops 4096 | bytes 24576 | tf_op jit(solution)/shard_map/convert_element_type | solution.py:493

commit v5 on v4

--- a/solution.py
+++ b/solution.py
@@ -200,8 +200,8 @@
     hbm, out_ref = refs[:names], refs[names]
     local = refs[names + 1 : 2 * names + 1]
     (
-        load_sem, hv_send, hv_recv, rows_buf, part, res_buf, x_buf, y_send, y_recv,
-        hv_ss, hv_rs, part_ss, part_rs, x_ss, x_rs, f_ss, f_rs, y_ss, y_rs,
+        load_sem, hv_send, hv_recv, rows_buf, part, res_buf, x_buf, y_send, p_recv, z_buf, y_recv,
+        hv_ss, hv_rs, part_ss, part_rs, x_ss, x_rs, f_ss, f_rs, p_ss, p_rs, y_ss, y_rs,
     ) = refs[2 * names + 1 :]
     (
         hidden, attn_gain, w_qdown, q_gain, w_qnope, w_qrope, w_kvdown, kv_gain, w_krope,
@@ -209,8 +209,6 @@
         route_weights, w_gate, w_up, w_down, inverse,
     ) = local
     g, t = lax.axis_index("ep"), lax.axis_index("tp")
-    devices = groups * lanes_tp
-    me = g * lanes_tp + t
 
     barrier = pltpu.get_barrier_semaphore()
 
@@ -390,9 +388,21 @@
         gate = gate + mm_nt(piece, w_gate[0, :, depth])
         up = up + mm_nt(piece, w_up[0, :, depth])
     inner = (gate / (1.0 + jnp.exp(-gate)) * up).astype(BF16)
-    for i in range(lanes_tp):
-        term = mm(inner, w_down[0, :, i * quarter : (i + 1) * quarter]).astype(BF16)
-        y_send[:, i] = term.reshape(groups, rows, quarter)
+    pairs = lanes_tp // 2
+
+    def p_copy(j):
+        return pltpu.make_async_remote_copy(
+            y_send.at[0, j], p_recv.at[j], p_ss.at[j], p_rs.at[j],
+            device_id=(g, partner), device_id_type=LINK,
+        )
+
+    for k, parity in enumerate((1 - mine_half, mine_half)):
+        for j in range(pairs):
+            start = pl.multiple_of((2 * j + parity) * quarter, quarter)
+            term = mm(inner, w_down[0, :, pl.ds(start, quarter)]).astype(BF16)
+            y_send[k, j] = term.reshape(groups, rows, quarter)
+            if k == 0:
+                p_copy(j).start()
 
     same = iota((rows, rows), 0) == iota((rows, rows), 1)
     weights = []
@@ -402,35 +412,31 @@
         )
         weights.append(jnp.sum(jnp.where(same, flat, 0.0), axis=1, keepdims=True))
 
-    def y_copy(other_g, other_t, slot_g, slot_t):
+    chip = t // 2
+
+    def y_copy(other, j, slot_g, slot_j):
         return pltpu.make_async_remote_copy(
-            y_send.at[other_g, other_t], y_recv.at[slot_g, slot_t],
-            y_ss.at[other_g, other_t], y_rs.at[slot_g, slot_t],
-            device_id=(other_g, other_t), device_id_type=LINK,
-        )
-
-    def spread(step):
-        peer = lax.rem(me + step, devices)
-        return peer // lanes_tp, lax.rem(peer, lanes_tp)
-
-    def y_start(step, carry):
-        a, b = spread(step)
-        y_copy(a, b, g, t).start()
-        return carry
-
-    lax.fori_loop(1, devices, y_start, 0)
-    y_recv[g, t] = y_send[g, t]
-
-    def y_wait(step, carry):
-        a, b = spread(step)
+            z_buf.at[j, other], y_recv.at[slot_g, slot_j],
+            y_ss.at[other, j], y_rs.at[slot_g, slot_j],
+            device_id=(other, 2 * j + mine_half), device_id_type=LINK,
+        )
+
+    for j in range(pairs):
+        p_copy(j).wait_recv()
+        z_buf[j] = (y_send[1, j].astype(F32) + p_recv[j].astype(F32)).astype(BF16)
+    spread = [
+        (lax.rem(g + i, groups), lax.rem(chip + j, pairs))
+        for i in range(groups) for j in range(pairs)
+    ][1:]
+    for a, b in spread:
+        y_copy(a, b, g, chip).start()
+    y_recv[g, chip] = z_buf[chip, g]
+    for a, b in spread[::-1]:
         y_copy(a, b, a, b).wait_recv()
-        return carry
-
-    lax.fori_loop(1, devices, y_wait, 0)
     total = res_buf[t]
     for u in range(groups):
         half = y_recv[u, 0].astype(F32)
-        for i in range(1, lanes_tp):
+        for i in range(1, pairs):
             half = half + y_recv[u, i].astype(F32)
         total = total + weights[u // 2] * half.astype(BF16).astype(F32)
     out_ref[...] = total
@@ -441,12 +447,10 @@
 
     x_sends_done()
 
-    def y_done(step, carry):
-        a, b = spread(step)
-        y_copy(a, b, g, t).wait_send()
-        return carry
-
-    lax.fori_loop(1, devices, y_done, 0)
+    for j in range(pairs):
+        p_copy(j).wait_send()
+    for a, b in spread:
+        y_copy(a, b, g, chip).wait_send()
 
 
 def fused_layer(groups, lanes_tp, *args):
@@ -481,11 +485,14 @@
             pltpu.VMEM((lanes_tp, rows, width), BF16),
             pltpu.VMEM((lanes_tp, rows, quarter), F32),
             pltpu.VMEM((groups, 2, rows, width // 2), BF16),
-            pltpu.VMEM((groups, lanes_tp, rows, quarter), BF16),
-            pltpu.VMEM((groups, lanes_tp, rows, quarter), BF16),
+            pltpu.VMEM((2, lanes_tp // 2, groups, rows, quarter), BF16),
+            pltpu.VMEM((lanes_tp // 2, groups, rows, quarter), BF16),
+            pltpu.VMEM((lanes_tp // 2, groups, rows, quarter), BF16),
+            pltpu.VMEM((groups, lanes_tp // 2, rows, quarter), BF16),
             sem((lanes_tp,)), sem((lanes_tp,)), sem((lanes_tp,)), sem((lanes_tp,)),
             sem((groups,)), sem((groups,)), sem((groups,)), sem((groups,)),
-            sem((groups, lanes_tp)), sem((groups, lanes_tp)),
+            sem((lanes_tp // 2,)), sem((lanes_tp // 2,)),
+            sem((groups, lanes_tp // 2)), sem((groups, lanes_tp // 2)),
         ],
         compiler_params=pltpu.CompilerParams(
             collective_id=0, has_side_effects=True, vmem_limit_bytes=60 * 1024 * 1024

time: 29.8 us -> 28.3 us (0.950)
  Pallas kernels: 28.8 us -> 27.6 us
    pallas_call x1, Pallas kernels: 28.8 us -> 27.6 us  [fused_layer(): pl.pallas_call(functools.partial(layer_kernel, groups, lanes_tp), out_sha...]
where the time goes in v5:
time: 28.3 us; the launch traced here: 28.2 us
  Pallas kernels  27.6 us (98%)
  other arithmetic  0.6 us (2%)
    pallas_call x1, Pallas kernels, fused_layer(): pl.pallas_call(functools.partial(layer_kernel, groups, lanes_tp), out_sha...  27.6 us
    convert_element_type x1, other arithmetic, fused_layer(): return pl.pallas_call(functools.partial(layer_kernel, groups, lanes_tp),...  0.6 us

profile of v5, /device:TPU:0, one launch (start us, length us, event | category | flops | bytes accessed | tf_op | source)
XLA Modules:
  0.0 28.2 jit_solution(5409632781733360643)
XLA Ops:
  0.0 27.6 %shard_map.208 = f32[16,256]{1,0:T(8,128)S(1)} custom-call(bf16[16,1024]{1,0:T(8,128)(2,1)} %refs_0_.1, f32[1,1024]{1,0:T(1,128)} %bitcast.12, bf16[1024,256]{1,0:T(8,128)(2,1)} %refs_2_.1, f32[1,256]{1,0:T(1,128)} %bitcast.14, bf16[256,512]{1,0:T(8,128)(2,1)} %refs_4_.1, bf16[256,256]{1,0:T(8,128)(2,1)} %refs_5_.1, bf16[1024,128]{1,0:T(8,128)(2,1)} %refs_6_.1, ...), custom_call_target="tpu_custom_call" | custom-call | tf_op jit(solution)/shard_map/pallas_call | solution.py:474
  27.6 0.6 %convert_element_type.3 = bf16[16,256]{1,0:T(8,128)(2,1)} convert(f32[16,256]{1,0:T(8,128)S(1)} %shard_map.208) | non-fusion elementwise | flops 4096 | bytes 24576 | tf_op jit(solution)/shard_map/convert_element_type | solution.py:500
